TPU v7x, 32 devices: a whole 2x2x4 slice. The times are simulated.
32 devices in a mesh: ep: 8 (over z, y), tp: 4 (over x, core).
Axes of the slice: x: 2, y: 2, z: 4, core: 2. Of those that a mesh axis runs over, the one named last changes fastest.
Arguments:
- c_gate: bfloat16 [2048, 1024], P('ep', 'tp'), may hold values from -6 to 6
- b_gate: bfloat16 [2048, 1024], P('ep', 'tp'), may hold values from -6 to 6
- values: bfloat16 [2048, 1024], P('ep', 'tp'), may hold values from -6 to 6
- conv_taps: float32 [3, 1024], P(None, 'tp'), may hold values from -3.5 to 3.5
- w_mix_out: bfloat16 [1024, 2048], P('tp'), may hold values from -0.1875 to 0.1875
- moe_in: bfloat16 [4096, 2048], P(('ep', 'tp')), may hold values from -6 to 6
- norm_gain: float32 [2048], replicated, may hold values from 0.1 to 1.9
- route_ids: int32 [4096, 2], P(('ep', 'tp')), may hold values from 0 to 7, all different within a row; in each aligned block of 128 rows (0 to 127, 128 to 255, ...) at most 40 rows name the same one
- route_weights: float32 [4096, 2], P(('ep', 'tp')), may hold values from 0.1 to 1
- w_gate: bfloat16 [8, 2048, 3584], P('ep', None, 'tp'), may hold values from -0.125 to 0.125
- w_up: bfloat16 [8, 2048, 3584], P('ep', None, 'tp'), may hold values from -0.125 to 0.125
- w_down: bfloat16 [8, 3584, 2048], P('ep', 'tp'), may hold values from -0.09375 to 0.09375
Outputs:
- mixer_out: bfloat16 [2048, 2048], P(('ep', 'tp'))
- moe_out: bfloat16 [4096, 2048], P(('ep', 'tp'))
Inputs may be any that keep to these rules, and one draw needn't show every extreme that they name: `route_ids`: each row names 2 different experts; in each aligned block of 128 rows (the rows of one device) no expert is named by more than 40 rows, and in every draw some expert is named by exactly 40 rows in some block.
All inputs are finite; a program needn't handle non-finite values.
Results may differ from a plain program's by a relative error of at most 0.012.
Values may be sent and summed in bfloat16 or wider, within the bound.
A program may use at most 128 MiB of HBM per device.

v0:
```python
import jax
import jax.numpy as jnp
from jax import lax
from jax.sharding import PartitionSpec as P

EPS = 1e-06


def passed_along(block, axis, distance):
    devices = range(lax.axis_size(axis))
    route = [(i - distance, i) for i in devices if i - distance in devices]
    return lax.ppermute(block, axis, route)


def rank_copies(route_block, experts):
    flat_ids = route_block.reshape(-1)
    onehot = (flat_ids[:, None] == jnp.arange(experts, dtype=jnp.int32)[None, :]).astype(jnp.int32)
    before = jnp.cumsum(onehot, axis=0) - onehot
    return (flat_ids, jnp.sum(before * onehot, axis=1))


def pack_rows(rows, slot_of, top, slot_count):
    copies = slot_of.shape[0]
    table = (
        jnp.full((slot_count,), copies, jnp.int32)
        .at[slot_of]
        .set(jnp.arange(copies, dtype=jnp.int32))
    )
    padded = jnp.concatenate([rows, jnp.zeros((1, rows.shape[1]), rows.dtype)], 0)
    return padded[table // top]


def on_device(
    c_gate,
    b_gate,
    values,
    conv_taps,
    w_mix_out,
    moe_in,
    norm_gain,
    route_ids,
    route_weights,
    w_gate,
    w_up,
    w_down,
):
    tokens = c_gate.shape[0]
    reach = conv_taps.shape[0] - 1
    product = c_gate.astype(jnp.float32) * values.astype(jnp.float32)
    previous = passed_along(product[tokens - reach :], "ep", 1)
    extended = jnp.concatenate([previous, product], 0)
    convolved = jnp.zeros_like(product)
    for offset in range(reach + 1):
        convolved = convolved + conv_taps[offset][None, :] * extended[offset : offset + tokens]
    mixed = (b_gate.astype(jnp.float32) * convolved).astype(jnp.bfloat16)
    piece = mixed
    mixer_out = lax.psum_scatter(
        jnp.dot(piece, w_mix_out, preferred_element_type=jnp.float32).astype(jnp.bfloat16),
        "tp",
        scatter_dimension=0,
        tiled=True,
    )
    rows_b = moe_in.shape[0]
    width = moe_in.shape[1]
    top = route_ids.shape[1]
    n_ep = lax.axis_size("ep")
    experts = w_gate.shape[0] * n_ep
    capacity = 5 * rows_b * top // (4 * experts)
    stream = moe_in.astype(jnp.float32)
    scale = lax.rsqrt(jnp.mean(stream * stream, axis=1, keepdims=True) + EPS)
    normed = (stream * scale * norm_gain[None, :]).astype(jnp.bfloat16)
    own_ids, own_ranks = rank_copies(route_ids, experts)
    own_slot = own_ids * capacity + own_ranks
    outgoing = pack_rows(normed, own_slot, top, experts * capacity).reshape(
        experts, capacity, width
    )
    arrived = lax.all_to_all(outgoing, "ep", split_axis=0, concat_axis=1, tiled=True).reshape(
        -1, width
    )
    piece = lax.all_gather(arrived, "tp", axis=0, tiled=True)
    gate_val = jnp.dot(piece, w_gate[0], preferred_element_type=jnp.float32)
    up_val = jnp.dot(piece, w_up[0], preferred_element_type=jnp.float32)
    hidden = (jax.nn.silu(gate_val) * up_val).astype(jnp.bfloat16)
    piece = hidden
    expert_out = lax.psum_scatter(
        jnp.dot(piece, w_down[0], preferred_element_type=jnp.float32).astype(jnp.bfloat16),
        "tp",
        scatter_dimension=0,
        tiled=True,
    )
    returned = lax.all_to_all(
        expert_out.reshape(n_ep, capacity, width), "ep", split_axis=0, concat_axis=0, tiled=True
    )
    picked = returned.reshape(-1, width)[own_slot].astype(jnp.float32).reshape(rows_b, top, width)
    moe_out = jnp.sum(picked * route_weights[:, :, None], axis=1).astype(jnp.bfloat16)
    return (mixer_out, moe_out)


def solution(mesh):
    return jax.shard_map(
        on_device,
        mesh=mesh,
        in_specs=(
            P("ep", "tp"),
            P("ep", "tp"),
            P("ep", "tp"),
            P(None, "tp"),
            P("tp", None),
            P(("ep", "tp"), None),
            P(),
            P(("ep", "tp"), None),
            P(("ep", "tp"), None),
            P("ep", None, "tp"),
            P("ep", None, "tp"),
            P("ep", "tp", None),
        ),
        out_specs=(P(("ep", "tp"), None), P(("ep", "tp"), None)),
        check_vma=False,
    )
```

profile of v0, /device:TPU:0, one launch (start us, length us, event | category | flops | bytes accessed | tf_op | source)
XLA Modules:
  0.0 225.9 jit_solution(5332753036802523370)
XLA Ops:
  7.2 0.0 copy-start
  7.2 0.0 all-gather.2.cloned.1.call-start
  7.2 0.9 copy.16
  8.1 0.1 eq.29
  8.2 0.1 eq.25
  8.4 0.7 broadcast_multiply_fusion
  9.1 0.6 reduce-window.6
  9.6 0.2 slice_reduce_fusion
  9.9 0.1 copy.15
  10.0 0.1 mul.107
  10.1 0.1 fusion.19
  10.3 1.4 scatter_custom_fusion
  11.7 1.2 fusion.4
  12.9 1.2 fusion.6
  14.2 2.4 %gather_fusion = bf16[320,2048]{1,0:T(8,128)(2,1)S(1)} fusion(bf16[129,2048]{1,0:T(8,128)(2,1)S(1)} %concatenate.7, s32[1024]{0:T(1024)S(1)} %pad_clamp_fusion.1), kind=kCustom, calls=%fused_computation | custom fusion | bytes 2622720 | tf_op jit(solution)/shard_map/gather | solution.py:30
  16.7 38.6 %all_to_all.14 = bf16[8,40,2048]{2,1,0:T(8,128)(2,1)} all-to-all(bf16[8,40,2048]{2,1,0:T(8,128)(2,1)S(1)} %bitcast.39), channel_id=1, replica_groups=mesh['ep'=8,'tp'=4] {'ep'}, dimensions={0} | all-to-all | bytes 2621440 | tf_op jit(solution)/shard_map/all_to_all | solution.py:77
  55.3 0.0 all-gather.2.cloned.1.call-update
  55.3 0.0 reduce-scatter.5.cloned.1.call-start
  55.3 39.5 %all-gather.2.cloned.1.call-done = bf16[1280,2048]{1,0:T(8,128)(2,1)} async-done(((bf16[320,2048]{1,0:T(8,128)(2,1)}), bf16[1280,2048]{1,0:T(8,128)(2,1)}) %all-gather.2.cloned.1.call-update) | async-done | bytes 5242896 | tf_op jit(solution)/shard_map/all_gather | solution.py:80
  94.9 10.0 %fusion.2 = f32[1280,896]{1,0:T(8,128)} fusion(bf16[1280,2048]{1,0:T(8,128)(2,1)} %all-gather.2.cloned.1.call-done, bf16[1,2048,896]{2,1,0:T(8,128)(2,1)} %param.21), kind=kOutput, calls=%fused_computation.7 | convolution fusion | flops 4697620480 | bytes 13500416 | tf_op jit(solution)/shard_map/dot_general | solution.py:81
  104.8 17.6 %convolution_convert_fusion = bf16[1280,2048]{1,0:T(8,128)(2,1)} fusion(bf16[1,896,2048]{2,1,0:T(8,128)(2,1)} %param.23, f32[1280,896]{1,0:T(8,128)} %fusion.2, bf16[1280,2048]{1,0:T(8,128)(2,1)} %all-gather.2.cloned.1.call-done, bf16[1,2048,896]{2,1,0:T(8,128)(2,1)} %param.22), kind=kOutput, calls=%fused_computation.3 | convolution fusion | flops 9404743680 | bytes 22413312 | tf_op jit(solution)/shard_map/dot_general | solution.py:86
  122.4 0.0 copy-start.2
  122.4 0.0 copy-start.3
  122.4 0.0 copy-start.4
  122.4 0.0 copy-start.1
  122.4 0.0 reduce-scatter.5.cloned.1.call-update
  122.4 0.9 copy-done.2
  123.3 0.1 copy-done.3
  123.4 0.0 copy-start.5
  123.4 3.4 %collective-permute-start = (f32[2,256]{1,0:T(2,128)S(1)}, f32[2,256]{1,0:T(2,128)S(1)}, u32[]{:S(2)}, u32[]{:S(2)}) collective-permute-start(f32[2,256]{1,0:T(2,128)S(1)} %slice.36), channel_id=1, source_target_pairs={{0,4},{4,8},{8,12},{12,16},{16,20},{20,24},{24,28},{1,5},{5,9},{9,... | collective-permute-start | bytes 6152 | tf_op jit(solution)/shard_map/ppermute | solution.py:12
  126.8 47.2 %reduce-scatter.5.cloned.1.call-done = bf16[320,2048]{1,0:T(8,128)(2,1)} async-done(((bf16[1280,2048]{1,0:T(8,128)(2,1)}), bf16[320,2048]{1,0:T(8,128)(2,1)}) %reduce-scatter.5.cloned.1.call-update) | async-done | bytes 1310736 | tf_op jit(solution)/shard_map/reduce_scatter | solution.py:85
  174.0 5.5 %all-to-all-start.1 = ((bf16[8,40,2048]{2,1,0:T(8,128)(2,1)}), bf16[8,40,2048]{2,1,0:T(8,128)(2,1)S(1)}, u32[]{:S(2)}, u32[]{:S(2)}) async-start(bf16[8,40,2048]{2,1,0:T(8,128)(2,1)} %bitcast.41), calls=%async_computation.3 | async-start | bytes 2621440 | tf_op jit(solution)/shard_map/all_to_all | solution.py:91
  179.5 0.2 reduce-scatter.3.cloned.1.call-start
  179.7 0.0 copy-done.4
  179.7 0.0 collective-permute-done
  179.7 0.0 copy-done
  179.7 0.0 copy-done.1
  179.8 1.5 convolution_convert_fusion.1
  181.2 0.0 reduce-scatter.3.cloned.1.call-update
  181.2 0.0 copy-done.5
  181.3 0.1 copy.18
  181.4 29.3 %all-to-all-done.1 = bf16[8,40,2048]{2,1,0:T(8,128)(2,1)S(1)} async-done(((bf16[8,40,2048]{2,1,0:T(8,128)(2,1)}), bf16[8,40,2048]{2,1,0:T(8,128)(2,1)S(1)}, u32[]{:S(2)}, u32[]{:S(2)}) %all-to-all-start.1) | async-done | bytes 1310752 | tf_op jit(solution)/shard_map/all_to_all | solution.py:91
  210.7 2.3 %gather_fusion.1 = bf16[256,2048]{1,0:T(8,128)(2,1)} fusion(bf16[320,2048]{1,0:T(8,128)(2,1)S(1)} %bitcast.38, s32[1024]{0:T(1024)S(1)} %pad_clamp_fusion), kind=kCustom, calls=%fused_computation.1 | custom fusion | bytes 2098176 | tf_op jit(solution)/shard_map/gather | solution.py:94
  213.0 2.4 %reshape.85 = f32[128,2,2048]{2,1,0:T(2,128)S(1)} reshape(bf16[256,2048]{1,0:T(8,128)(2,1)} %gather_fusion.1) | data formatting | bytes 3145728 | tf_op jit(solution)/shard_map/convert_element_type | solution.py:94
  215.4 3.9 %multiply_reduce_fusion = bf16[128,2048]{1,0:T(8,128)(2,1)} fusion(f32[128,2,2048]{2,1,0:T(2,128)S(1)} %reshape.85, f32[128,2]{1,0:T(8,128)S(1)} %copy.18), kind=kLoop, calls=%fused_computation.10 | loop fusion | flops 786432 | bytes 2622464 | tf_op jit(solution)/shard_map/reduce_sum | solution.py:95
  219.3 0.0 reduce-scatter.3.cloned.1.call-done
  (13 shorter events, 0.2 us)
Async XLA Ops:
  7.2 172.6 %copy-start = (bf16[256,2048]{1,0:T(8,128)(2,1)S(1)}, bf16[256,2048]{1,0:T(8,128)(2,1)}, u32[]{:S(2)}) copy-start(bf16[256,2048]{1,0:T(8,128)(2,1)} %param.16) | copy-start | bytes 3145732
  7.2 87.7 %all-gather.2.cloned.1.call-start = ((), (), s32[]{:S(2)}) async-start(), calls=%async_computation.5 | async-start | bytes 6553600 | tf_op jit(solution)/shard_map/all_gather | solution.py:80
  55.3 118.7 %reduce-scatter.5.cloned.1.call-start = ((), (), s32[]{:S(2)}) async-start(), calls=%async_computation.6 | async-start | bytes 6553600 | tf_op jit(solution)/shard_map/reduce_scatter | solution.py:85
  122.4 0.9 copy-start.2
  122.4 1.0 copy-start.3
  122.4 57.3 %copy-start.4 = (f32[3,256]{1,0:T(4,128)S(1)}, f32[3,256]{1,0:T(4,128)}, u32[]{:S(2)}) copy-start(f32[3,256]{1,0:T(4,128)} %param.15) | copy-start | bytes 9220
  122.4 57.3 %copy-start.1 = (bf16[256,256]{1,0:T(8,128)(2,1)S(1)}, bf16[256,256]{1,0:T(8,128)(2,1)}, u32[]{:S(2)}) copy-start(bf16[256,256]{1,0:T(8,128)(2,1)} %param.13) | copy-start | bytes 393220
  123.4 57.9 %copy-start.5 = (f32[128,2]{0,1:T(2,128)S(1)}, f32[128,2]{0,1:T(2,128)}, u32[]{:S(2)}) copy-start(f32[128,2]{0,1:T(2,128)} %param.20) | copy-start | bytes 3076
  123.4 56.3 %collective-permute-start = (f32[2,256]{1,0:T(2,128)S(1)}, f32[2,256]{1,0:T(2,128)S(1)}, u32[]{:S(2)}, u32[]{:S(2)}) collective-permute-start(f32[2,256]{1,0:T(2,128)S(1)} %slice.36), channel_id=1, source_target_pairs={{0,4},{4,8},{8,12},{12,16},{16,20},{20,24},{24,28},{1,5},{5,9},{9,... | collective-permute-start | bytes 6152 | tf_op jit(solution)/shard_map/ppermute | solution.py:12
  174.0 36.7 %all-to-all-start.1 = ((bf16[8,40,2048]{2,1,0:T(8,128)(2,1)}), bf16[8,40,2048]{2,1,0:T(8,128)(2,1)S(1)}, u32[]{:S(2)}, u32[]{:S(2)}) async-start(bf16[8,40,2048]{2,1,0:T(8,128)(2,1)} %bitcast.41), calls=%async_computation.3 | async-start | bytes 2621440 | tf_op jit(solution)/shard_map/all_to_all | solution.py:91
  179.5 39.9 %reduce-scatter.3.cloned.1.call-start = ((), (), s32[]{:S(2)}) async-start(), calls=%async_computation.4 | async-start | bytes 1310720 | tf_op jit(solution)/shard_map/reduce_scatter | solution.py:57
Sparse Core Ops, SparseCore 0:
  55.4 39.4 all-gather.1
  122.6 51.3 reduce-scatter.4
  183.4 25.2 reduce-scatter.2
where the time goes:
time: 226 us
  waiting for transfers between devices  116 us (51%)
  blocking collectives  38.6 us (17%)
  matrix products  29 us (13%)
  between operations  13.9 us (6%)
  local copies, waits for them, and re-layouts  11.3 us (5%)
  starting transfers between devices  9.19 us (4%)
  other arithmetic  7.85 us (3%)
    reduce_scatter x1, waiting for transfers between devices, on_device(): lax.psum_scatter(jnp.dot(piece, w_down[0], preferred_element_type=jnp.flo...  47.2 us
    all_gather x1, waiting for transfers between devices, on_device(): piece = lax.all_gather(arrived, 'tp', axis=0, tiled=True)  39.5 us
    all_to_all x1, blocking collectives, on_device(): lax.all_to_all(outgoing, 'ep', split_axis=0, concat_axis=1, tiled=True)  38.6 us
    all_to_all x1, waiting for transfers between devices, on_device(): lax.all_to_all(expert_out.reshape(n_ep, capacity, width), 'ep', split_axi...  29.3 us
    dot_general x1, matrix products, on_device(): jnp.dot(piece, w_down[0], preferred_element_type=jnp.float32)  17.6 us
    dot_general x1, matrix products, on_device(): gate_val = jnp.dot(piece, w_gate[0], preferred_element_type=jnp.float32)  9.98 us
    all_to_all x1, starting transfers between devices, on_device(): lax.all_to_all(expert_out.reshape(n_ep, capacity, width), 'ep', split_axi...  5.52 us
  transfers between devices with their start and end apart: 5, of which 3 were waited for; matrix products, arithmetic and copies ran while one was open for 5% of the time, Pallas kernels for 0%

commit v1 on v0

v1 whole, which is shorter than its diff:
```python
import functools

import jax
import jax.numpy as jnp
from jax import lax
from jax.experimental import pallas as pl
from jax.experimental.pallas import tpu as pltpu
from jax.sharding import PartitionSpec as P

EPS = 1e-06
PAIRS = 4
MESH = pl.DeviceIdType.MESH


def passed_along(block, axis, distance):
    devices = range(lax.axis_size(axis))
    route = [(i - distance, i) for i in devices if i - distance in devices]
    return lax.ppermute(block, axis, route)


def remote(src, dst, send_sem, recv_sem, ep, tp):
    return pltpu.make_async_remote_copy(
        src_ref=src,
        dst_ref=dst,
        send_sem=send_sem,
        recv_sem=recv_sem,
        device_id=(ep, tp),
        device_id_type=MESH,
    )


def places():
    ep = lax.axis_index("ep")
    tp = lax.axis_index("tp")
    partner = tp + 1 - 2 * (tp % 2)
    across = (tp + 2) % PAIRS
    diagonal = (partner + 2) % PAIRS
    return ep, tp, partner, across, diagonal


def greet(n, ep, tp, partner, across):
    barrier = pltpu.get_barrier_semaphore()

    def hello(s, carry):
        pl.semaphore_signal(
            barrier, inc=1, device_id=((ep + s) % n, tp), device_id_type=MESH
        )
        return carry

    lax.fori_loop(1, n, hello, 0)
    pl.semaphore_signal(barrier, inc=1, device_id=(ep, partner), device_id_type=MESH)
    pl.semaphore_signal(barrier, inc=1, device_id=(ep, across), device_id_type=MESH)
    pl.semaphore_wait(barrier, n + 1)


def loop(lower, upper, body):
    lax.fori_loop(lower, upper, lambda s, carry: (body(s), carry)[1], 0)


def dispatch_kernel(
    n, own, all_rows, a_send, a_recv, c_send, c_recv, x_send, x_recv, r_send, r_recv, local_sem
):
    ep, tp, partner, across, diagonal = places()
    local = pltpu.make_async_copy(own.at[ep], all_rows.at[tp, ep], local_sem)
    local.start()
    greet(n, ep, tp, partner, across)

    def to_expert(s):
        to = (ep + s) % n
        return remote(own.at[to], all_rows.at[tp, ep], a_send.at[s], a_recv.at[s], to, tp)

    def from_source(s):
        to = (ep + s) % n
        return remote(
            own.at[to], all_rows.at[tp, (ep + n - s) % n], a_send.at[s], a_recv.at[s], to, tp
        )

    def shared(s, row, sends, recvs, to):
        block = all_rows.at[row, (ep + n - s) % n]
        return remote(block, block, sends.at[s], recvs.at[s], ep, to)

    loop(1, n, lambda s: to_expert(s).start())
    local.wait()

    def share(s):
        shared(s, tp, x_send, x_recv, across).start()
        shared(s, tp, c_send, c_recv, partner).start()

    share(0)

    def arrive(s):
        from_source(s).wait_recv()
        share(s)

    loop(1, n, arrive)

    def relay(s):
        shared(s, across, x_send, x_recv, across).wait_recv()
        shared(s, across, r_send, r_recv, partner).start()

    loop(0, n, relay)

    def finish(s):
        shared(s, tp, x_send, x_recv, across).wait_send()
        shared(s, tp, c_send, c_recv, partner).wait_send()
        shared(s, partner, c_send, c_recv, partner).wait_recv()
        shared(s, across, r_send, r_recv, partner).wait_send()
        shared(s, diagonal, r_send, r_recv, partner).wait_recv()

    loop(0, n, finish)
    loop(1, n, lambda s: to_expert(s).wait_send())


def added(*blocks):
    total = blocks[0].astype(jnp.float32)
    for block in blocks[1:]:
        total = total + block.astype(jnp.float32)
    return total.astype(jnp.bfloat16)


def combine_kernel(
    n,
    parts,
    mix_parts,
    back,
    mix_out,
    c_in,
    x_out,
    x_in,
    done,
    mc_in,
    mx_out,
    mx_in,
    c_send,
    c_recv,
    d_send,
    d_recv,
    x_send,
    x_recv,
    a_send,
    a_recv,
    m_send,
    m_recv,
):
    ep, tp, partner, across, diagonal = places()
    greet(n, ep, tp, partner, across)

    def to_of(s):
        return (ep + 1 + s) % n

    def far(s):
        return remote(
            parts.at[diagonal, to_of(s)], c_in.at[1, s], d_send.at[s], d_recv.at[s], ep, partner
        )

    def near(s):
        return remote(
            parts.at[partner, to_of(s)], c_in.at[0, s], c_send.at[s], c_recv.at[s], ep, partner
        )

    def cross(s):
        return remote(x_out.at[s], x_in.at[s], x_send.at[s], x_recv.at[s], ep, across)

    def home(s):
        return remote(done.at[s], back.at[ep], a_send.at[s], a_recv.at[s], to_of(s), tp)

    def home_arrived(s):
        return remote(
            done.at[s],
            back.at[(ep + n - 1 - s) % n],
            a_send.at[s],
            a_recv.at[s],
            to_of(s),
            tp,
        )

    m_far = remote(mix_parts.at[diagonal], mc_in.at[1], m_send.at[0], m_recv.at[0], ep, partner)
    m_near = remote(mix_parts.at[partner], mc_in.at[0], m_send.at[1], m_recv.at[1], ep, partner)
    m_cross = remote(mx_out, mx_in, m_send.at[2], m_recv.at[2], ep, across)

    loop(0, n, lambda s: far(s).start())
    m_far.start()
    loop(0, n, lambda s: near(s).start())
    m_near.start()

    def first_sum(s):
        far(s).wait_recv()
        x_out[s] = added(parts[across, to_of(s)], c_in[1, s])
        cross(s).start()

    loop(0, n, first_sum)
    m_far.wait_recv()
    mx_out[...] = added(mix_parts[across], mc_in[1])
    m_cross.start()

    def second_sum(s):
        near(s).wait_recv()
        cross(s).wait_recv()
        return added(parts[tp, to_of(s)], c_in[0, s], x_in[s])

    def send_home(s):
        done[s] = second_sum(s)
        home(s).start()

    loop(0, n - 1, send_home)
    back[ep] = second_sum(n - 1)
    m_near.wait_recv()
    m_cross.wait_recv()
    mix_out[...] = added(mix_parts[tp], mc_in[0], mx_in[...])

    def finish(s):
        far(s).wait_send()
        near(s).wait_send()
        cross(s).wait_send()

    loop(0, n, finish)

    def finish_home(s):
        home_arrived(s).wait_recv()
        home(s).wait_send()

    loop(0, n - 1, finish_home)
    m_far.wait_send()
    m_near.wait_send()
    m_cross.wait_send()


def dispatch(own, n):
    sems = [pltpu.SemaphoreType.DMA((n,))] * 8 + [pltpu.SemaphoreType.DMA]
    return pl.pallas_call(
        functools.partial(dispatch_kernel, n),
        out_shape=jax.ShapeDtypeStruct((PAIRS,) + own.shape, own.dtype),
        in_specs=[pl.BlockSpec(memory_space=pltpu.VMEM)],
        out_specs=pl.BlockSpec(memory_space=pl.ANY),
        scratch_shapes=sems,
        compiler_params=pltpu.CompilerParams(collective_id=0, has_side_effects=True),
        cost_estimate=pl.CostEstimate(
            flops=30_000_000_000, bytes_accessed=10_000_000, transcendentals=0
        ),
        name="dispatch",
    )(own)


def combine(parts, mix_parts, n):
    block = parts.shape[2:]
    mix_block = mix_parts.shape[1:]
    kind = parts.dtype
    vmem = pl.BlockSpec(memory_space=pltpu.VMEM)
    return pl.pallas_call(
        functools.partial(combine_kernel, n),
        out_shape=(
            jax.ShapeDtypeStruct((n,) + block, kind),
            jax.ShapeDtypeStruct(mix_block, kind),
        ),
        in_specs=[vmem, vmem],
        out_specs=(vmem, vmem),
        scratch_shapes=[
            pltpu.VMEM((2, n) + block, kind),
            pltpu.VMEM((n,) + block, kind),
            pltpu.VMEM((n,) + block, kind),
            pltpu.VMEM((n,) + block, kind),
            pltpu.VMEM((2,) + mix_block, kind),
            pltpu.VMEM(mix_block, kind),
            pltpu.VMEM(mix_block, kind),
        ]
        + [pltpu.SemaphoreType.DMA((n,))] * 8
        + [pltpu.SemaphoreType.DMA((3,))] * 2,
        compiler_params=pltpu.CompilerParams(collective_id=1, has_side_effects=True),
        name="combine",
    )(parts, mix_parts)


def on_device(
    c_gate,
    b_gate,
    values,
    conv_taps,
    w_mix_out,
    moe_in,
    norm_gain,
    route_ids,
    route_weights,
    w_gate,
    w_up,
    w_down,
):
    n_tp = lax.axis_size("tp")
    assert n_tp == PAIRS
    tokens = c_gate.shape[0]
    reach = conv_taps.shape[0] - 1
    product = c_gate.astype(jnp.float32) * values.astype(jnp.float32)
    previous = passed_along(product[tokens - reach :], "ep", 1)
    extended = jnp.concatenate([previous, product], 0)
    convolved = jnp.zeros_like(product)
    for offset in range(reach + 1):
        convolved = convolved + conv_taps[offset][None, :] * extended[offset : offset + tokens]
    mixed = (b_gate.astype(jnp.float32) * convolved).astype(jnp.bfloat16)
    mix_parts = jnp.dot(mixed, w_mix_out, preferred_element_type=jnp.float32).astype(jnp.bfloat16)
    mix_parts = mix_parts.reshape(n_tp, tokens // n_tp, -1)

    rows_b = moe_in.shape[0]
    width = moe_in.shape[1]
    top = route_ids.shape[1]
    n_ep = lax.axis_size("ep")
    experts = w_gate.shape[0] * n_ep
    capacity = 5 * rows_b * top // (4 * experts)
    stream = moe_in.astype(jnp.float32)
    scale = lax.rsqrt(jnp.mean(stream * stream, axis=1, keepdims=True) + EPS)
    normed = (stream * scale * norm_gain[None, :]).astype(jnp.bfloat16)

    expert_at = jnp.arange(experts, dtype=jnp.int32)[:, None]
    chosen = jnp.zeros((experts, rows_b), jnp.bool_)
    weight = jnp.zeros((experts, rows_b), jnp.float32)
    for j in range(top):
        match = route_ids[:, j][None, :] == expert_at
        chosen = chosen | match
        weight = weight + jnp.where(match, route_weights[:, j][None, :], 0.0)
    token_at = jnp.arange(rows_b, dtype=jnp.int32)
    earlier = (token_at[:, None] < token_at[None, :]).astype(jnp.bfloat16)
    rank = jnp.dot(
        chosen.astype(jnp.bfloat16), earlier, preferred_element_type=jnp.float32
    ).astype(jnp.int32)
    slot_at = jnp.arange(capacity, dtype=jnp.int32)[None, :, None]
    placed = (rank[:, None, :] == slot_at) & chosen[:, None, :]
    select = placed.astype(jnp.bfloat16).reshape(experts * capacity, rows_b)
    own = jnp.dot(select, normed, preferred_element_type=jnp.float32).astype(jnp.bfloat16)

    piece = dispatch(own.reshape(experts, capacity, width), n_ep).reshape(-1, width)
    gate_val = jnp.dot(piece, w_gate[0], preferred_element_type=jnp.float32)
    up_val = jnp.dot(piece, w_up[0], preferred_element_type=jnp.float32)
    hidden = (jax.nn.silu(gate_val) * up_val).astype(jnp.bfloat16)
    parts = jnp.dot(hidden, w_down[0], preferred_element_type=jnp.float32).astype(jnp.bfloat16)
    returned, mixer_out = combine(
        parts.reshape(n_tp, n_ep, capacity, width), mix_parts, n_ep
    )
    returned = returned.reshape(-1, width)

    spread = jnp.where(placed, weight[:, None, :], 0.0).reshape(experts * capacity, rows_b)
    high = lax.reduce_precision(spread, 8, 7)
    low = (spread - high).astype(jnp.bfloat16)
    over_slots = (((0,), (0,)), ((), ()))
    moe_out = lax.dot_general(
        high.astype(jnp.bfloat16), returned, over_slots, preferred_element_type=jnp.float32
    ) + lax.dot_general(low, returned, over_slots, preferred_element_type=jnp.float32)
    return (mixer_out, moe_out.astype(jnp.bfloat16))


def solution(mesh):
    return jax.shard_map(
        on_device,
        mesh=mesh,
        in_specs=(
            P("ep", "tp"),
            P("ep", "tp"),
            P("ep", "tp"),
            P(None, "tp"),
            P("tp", None),
            P(("ep", "tp"), None),
            P(),
            P(("ep", "tp"), None),
            P(("ep", "tp"), None),
            P("ep", None, "tp"),
            P("ep", None, "tp"),
            P("ep", "tp", None),
        ),
        out_specs=(P(("ep", "tp"), None), P(("ep", "tp"), None)),
        check_vma=False,
    )
```

time: 226 us -> 143 us (0.63)
  waiting for transfers between devices: 116 us -> 0.01 us
  Pallas kernels: 0 us -> 95.9 us
  blocking collectives: 38.6 us -> 0 us
  between operations: 13.9 us -> 0.76 us
  local copies, waits for them, and re-layouts: 11.3 us -> 1.58 us
  matrix products: 29 us -> 36.2 us
  other arithmetic: 7.85 us -> 2.45 us
  starting transfers between devices: 9.19 us -> 4.9 us
    pallas_call x0 -> x2, Pallas kernels: none -> 95.9 us  [the longest x1 49.4 us: combine(): pl.pallas_call(functools.partial(combine_kernel, n), out_shape=(jax.Shape...]
    reduce_scatter x2 -> x0, waiting for transfers between devices: 47.2 us -> none  [the longest x1 47.2 us: on_device(): lax.psum_scatter(jnp.dot(piece, w_down[0], preferred_element_type=jnp.flo...]
    all_gather x1 -> x0, waiting for transfers between devices: 39.5 us -> none  [on_device(): piece = lax.all_gather(arrived, 'tp', axis=0, tiled=True)]
    all_to_all x1 -> x0, blocking collectives: 38.6 us -> none  [on_device(): lax.all_to_all(outgoing, 'ep', split_axis=0, concat_axis=1, tiled=True)]
    all_to_all x1 -> x0, waiting for transfers between devices: 29.3 us -> none  [on_device(): lax.all_to_all(expert_out.reshape(n_ep, capacity, width), 'ep', split_axi...]
    dot_general x2 -> x6, matrix products: 19 us -> 26.3 us  [the longest x1 17.5 us: on_device(): jnp.dot(hidden, w_down[0], preferred_element_type=jnp.float32)]
    all_to_all x1 -> x0, starting transfers between devices: 5.52 us -> none  [on_device(): lax.all_to_all(expert_out.reshape(n_ep, capacity, width), 'ep', split_axi...]
    gather x2 -> x0, local copies, waits for them, and re-layouts: 4.78 us -> none  [the longest x1 2.44 us: pack_rows(): return padded[table // top]]
  transfers between devices with their start and end apart: 5 -> 1, of which waited for: 3 -> 0; matrix products, arithmetic and copies ran while one was open for 5% -> 23% of each run, Pallas kernels for 0% -> 33%
where the time goes in v1:
time: 143 us; the launch traced here: 142 us
  Pallas kernels  95.9 us (67%)
  matrix products  36.2 us (25%)
  starting transfers between devices  4.9 us (3%)
  other arithmetic  2.45 us (2%)
  local copies, waits for them, and re-layouts  1.58 us (1%)
    pallas_call x1, Pallas kernels, combine(): pl.pallas_call(functools.partial(combine_kernel, n), out_shape=(jax.Shape...  49.4 us
    pallas_call x1, Pallas kernels, dispatch(): pl.pallas_call(functools.partial(dispatch_kernel, n), out_shape=jax.Shape...  46.5 us
    dot_general x1, matrix products, on_device(): jnp.dot(hidden, w_down[0], preferred_element_type=jnp.float32)  17.5 us
    dot_general x1, matrix products, on_device(): gate_val = jnp.dot(piece, w_gate[0], preferred_element_type=jnp.float32)  9.97 us
    ppermute x1, starting transfers between devices, passed_along(): return lax.ppermute(block, axis, route)  4.9 us
  transfers between devices with their start and end apart: 1, of which 0 were waited for; matrix products, arithmetic and copies ran while one was open for 23% of the time, Pallas kernels for 33%

profile of v1, /device:TPU:0, one launch (start us, length us, event | category | flops | bytes accessed | tf_op | source)
XLA Modules:
  0.0 141.8 jit_solution(15793446834566187599)
XLA Ops:
  0.6 0.0 copy-start
  0.6 1.1 convert_multiply_fusion.2
  1.7 4.9 %collective-permute-start = (f32[2,256]{1,0:T(2,128)S(1)}, f32[2,256]{1,0:T(2,128)S(1)}, u32[]{:S(2)}, u32[]{:S(2)}) collective-permute-start(f32[2,256]{1,0:T(2,128)S(1)} %slice.40), channel_id=1, source_target_pairs={{0,4},{4,8},{8,12},{12,16},{16,20},{20,24},{24,28},{1,5},{5,9},{9,... | collective-permute-start | bytes 6152 | tf_op jit(solution)/shard_map/ppermute | solution.py:18
  6.7 0.8 slice_bitcast_fusion.3
  7.4 0.1 convolution_convert_fusion.3
  7.6 0.1 eq.82
  7.6 1.2 fusion.6
  8.9 0.1 fusion.21
  9.0 2.7 %convolution_convert_fusion.1 = bf16[320,2048]{1,0:T(8,128)(2,1)} fusion(pred[320,128]{1,0:T(32,128)(4,1)S(1)} %fusion.21, bf16[128,2048]{1,0:T(8,128)(2,1)} %param.17, f32[2048]{0:T(1024)} %param.18, f32[128]{0:T(128)S(1)} %add_rsqrt_fusion), kind=kOutput, calls=%fused_computation.6 | convolution fusion | flops 169476096 | bytes 1884672 | tf_op jit(solution)/shard_map/dot_general | solution.py:326
  11.7 0.0 copy-start.3
  11.7 0.0 copy-start.4
  11.7 46.5 %dispatch.1 = bf16[4,8,40,2048]{3,2,1,0:T(8,128)(2,1)} custom-call(bf16[8,40,2048]{2,1,0:T(8,128)(2,1)} %bitcast.55), custom_call_target="tpu_custom_call" | custom-call | flops 30000001024 | bytes 10000000 | tf_op jit(solution)/shard_map/dispatch/pallas_call | solution.py:230
  58.2 0.0 copy-done.3
  58.2 0.0 copy-done.4
  58.2 10.0 %fusion.2 = f32[1280,896]{1,0:T(8,128)} fusion(bf16[1280,2048]{1,0:T(8,128)(2,1)} %bitcast.59, bf16[1,2048,896]{2,1,0:T(8,128)(2,1)} %param.21), kind=kOutput, calls=%fused_computation.4 | convolution fusion | flops 4697620480 | bytes 13500416 | tf_op jit(solution)/shard_map/dot_general | solution.py:329
  68.2 0.0 copy-start.2
  68.2 17.5 %convolution_convert_fusion = bf16[1280,2048]{1,0:T(8,128)(2,1)} fusion(bf16[1,896,2048]{2,1,0:T(8,128)(2,1)} %param.23, f32[1280,896]{1,0:T(8,128)} %fusion.2, bf16[1280,2048]{1,0:T(8,128)(2,1)} %bitcast.60, bf16[1,2048,896]{2,1,0:T(8,128)(2,1)} %param.22), kind=kOutput, calls=%fused_computation | convolution fusion | flops 9404743680 | bytes 22413312 | tf_op jit(solution)/shard_map/dot_general | solution.py:332
  85.8 0.0 collective-permute-done
  85.8 0.0 copy-done
  85.8 0.0 copy-done.2
  85.8 1.5 %convolution_convert_fusion.2 = bf16[256,2048]{1,0:T(8,128)(2,1)} fusion(bf16[256,2048]{1,0:T(8,128)(2,1)S(1)} %copy-done, f32[2,256]{1,0:T(2,128)S(1)} %collective-permute-done, f32[256,256]{1,0:T(8,128)S(1)} %convert_multiply_fusion.2, bf16[256,256]{1,0:T(8,128)(2,1)S(1)} %copy-done.2, f32[256]{0:T(256)S(1)} %bitcast.57, f32[256]{0:T(256)S(1)} %bitcast.58, ...), kind=kOutput, calls=%fused_computation.7 | convolution fusion | flops 269615104 | bytes 2495488 | tf_op jit(solution)/shard_map/dot_general | solution.py:298
  87.2 49.4 %combine.1 = (bf16[8,40,2048]{2,1,0:T(8,128)(2,1)}, bf16[64,2048]{1,0:T(8,128)(2,1)}) custom-call(bf16[4,8,40,2048]{3,2,1,0:T(8,128)(2,1)} %bitcast.53, bf16[4,64,2048]{2,1,0:T(8,128)(2,1)} %bitcast.54), custom_call_target="tpu_custom_call" | custom-call | tf_op jit(solution)/shard_map/combine/pallas_call | solution.py:249
  136.6 0.0 copy-start.1
  136.7 1.9 %convolution_bitcast_fusion = f32[128,2048]{1,0:T(8,128)S(1)} fusion(bf16[8,40,2048]{2,1,0:T(8,128)(2,1)} %get-tuple-element.5, f32[8,128]{1,0:T(8,128)S(1)} %select_add_fusion, s32[8,128]{1,0:T(8,128)S(1)} %convolution_convert_fusion.3, pred[8,128]{1,0:T(8,128)(4,1)S(1)} %fusion.35), kind=kOutput, calls=%fused_computation.8 | convolution fusion | flops 168017920 | bytes 2368512 | tf_op jit(solution)/shard_map/dot_general | solution.py:344
  138.5 2.6 %fusion.5 = bf16[128,2048]{1,0:T(8,128)(2,1)} fusion(f32[128,2048]{1,0:T(8,128)S(1)} %convolution_bitcast_fusion, bf16[8,40,2048]{2,1,0:T(8,128)(2,1)} %get-tuple-element.5, f32[8,128]{1,0:T(8,128)S(1)} %select_add_fusion, s32[8,128]{1,0:T(8,128)S(1)} %convolution_convert_fusion.3, pred[8,128]{1,0:T(8,128)(4,1)S(1)} %fusion.35), kind=kOutput, calls=%fused_computation.11 | convolution fusion | flops 168501248 | bytes 2892800 | tf_op jit(solution)/shard_map/dot_general | solution.py:342
  141.1 0.0 copy-done.1
  141.1 0.7 copy.17
  (7 shorter events, 0.0 us)
Async XLA Ops:
  0.6 85.1 %copy-start = (bf16[256,2048]{1,0:T(8,128)(2,1)S(1)}, bf16[256,2048]{1,0:T(8,128)(2,1)}, u32[]{:S(2)}) copy-start(bf16[256,2048]{1,0:T(8,128)(2,1)} %param.16) | copy-start | bytes 3145732
  1.7 84.0 %collective-permute-start = (f32[2,256]{1,0:T(2,128)S(1)}, f32[2,256]{1,0:T(2,128)S(1)}, u32[]{:S(2)}, u32[]{:S(2)}) collective-permute-start(f32[2,256]{1,0:T(2,128)S(1)} %slice.40), channel_id=1, source_target_pairs={{0,4},{4,8},{8,12},{12,16},{16,20},{20,24},{24,28},{1,5},{5,9},{9,... | collective-permute-start | bytes 6152 | tf_op jit(solution)/shard_map/ppermute | solution.py:18
  11.7 46.5 %copy-start.3 = (f32[3,256]{1,0:T(4,128)S(1)}, f32[3,256]{1,0:T(4,128)}, u32[]{:S(2)}) copy-start(f32[3,256]{1,0:T(4,128)} %param.15) | copy-start | bytes 9220
  11.7 46.5 %copy-start.4 = (f32[128,2]{0,1:T(2,128)S(1)}, f32[128,2]{0,1:T(2,128)}, u32[]{:S(2)}) copy-start(f32[128,2]{0,1:T(2,128)} %param.20) | copy-start | bytes 3076
  68.2 17.6 %copy-start.2 = (bf16[256,256]{1,0:T(8,128)(2,1)S(1)}, bf16[256,256]{1,0:T(8,128)(2,1)}, u32[]{:S(2)}) copy-start(bf16[256,256]{1,0:T(8,128)(2,1)} %param.13) | copy-start | bytes 393220
  136.6 4.5 %copy-start.1 = (bf16[64,2048]{1,0:T(8,128)(2,1)S(1)}, bf16[64,2048]{1,0:T(8,128)(2,1)}, u32[]{:S(2)}) copy-start(bf16[64,2048]{1,0:T(8,128)(2,1)} %get-tuple-element.15) | copy-start | bytes 786436

commit v2 on v1

--- a/solution.py
+++ b/solution.py
@@ -10,12 +10,6 @@
 EPS = 1e-06
 PAIRS = 4
 MESH = pl.DeviceIdType.MESH
-
-
-def passed_along(block, axis, distance):
-    devices = range(lax.axis_size(axis))
-    route = [(i - distance, i) for i in devices if i - distance in devices]
-    return lax.ppermute(block, axis, route)
 
 
 def remote(src, dst, send_sem, recv_sem, ep, tp):
@@ -58,12 +52,29 @@
 
 
 def dispatch_kernel(
-    n, own, all_rows, a_send, a_recv, c_send, c_recv, x_send, x_recv, r_send, r_recv, local_sem
+    n,
+    own,
+    tail,
+    all_rows,
+    previous,
+    a_send,
+    a_recv,
+    c_send,
+    c_recv,
+    x_send,
+    x_recv,
+    r_send,
+    r_recv,
+    local_sem,
+    t_send,
+    t_recv,
 ):
     ep, tp, partner, across, diagonal = places()
     local = pltpu.make_async_copy(own.at[ep], all_rows.at[tp, ep], local_sem)
     local.start()
     greet(n, ep, tp, partner, across)
+    onward = remote(tail, previous, t_send, t_recv, (ep + 1) % n, tp)
+    onward.start()
 
     def to_expert(s):
         to = (ep + s) % n
@@ -92,13 +103,19 @@
         from_source(s).wait_recv()
         share(s)
 
-    loop(1, n, arrive)
-
     def relay(s):
         shared(s, across, x_send, x_recv, across).wait_recv()
         shared(s, across, r_send, r_recv, partner).start()
 
-    loop(0, n, relay)
+    lag = min(3, n - 1)
+
+    def arrive_and_relay(s):
+        arrive(s)
+        relay(s - lag)
+
+    loop(1, lag, arrive)
+    loop(lag, n, arrive_and_relay)
+    loop(n - lag, n, relay)
 
     def finish(s):
         shared(s, tp, x_send, x_recv, across).wait_send()
@@ -109,6 +126,7 @@
 
     loop(0, n, finish)
     loop(1, n, lambda s: to_expert(s).wait_send())
+    onward.wait()
 
 
 def added(*blocks):
@@ -225,20 +243,24 @@
     m_cross.wait_send()
 
 
-def dispatch(own, n):
-    sems = [pltpu.SemaphoreType.DMA((n,))] * 8 + [pltpu.SemaphoreType.DMA]
+def dispatch(own, tail, n):
+    sems = [pltpu.SemaphoreType.DMA((n,))] * 8 + [pltpu.SemaphoreType.DMA] * 3
+    vmem = pl.BlockSpec(memory_space=pltpu.VMEM)
     return pl.pallas_call(
         functools.partial(dispatch_kernel, n),
-        out_shape=jax.ShapeDtypeStruct((PAIRS,) + own.shape, own.dtype),
-        in_specs=[pl.BlockSpec(memory_space=pltpu.VMEM)],
-        out_specs=pl.BlockSpec(memory_space=pl.ANY),
+        out_shape=(
+            jax.ShapeDtypeStruct((PAIRS,) + own.shape, own.dtype),
+            jax.ShapeDtypeStruct(tail.shape, tail.dtype),
+        ),
+        in_specs=[vmem, vmem],
+        out_specs=(pl.BlockSpec(memory_space=pl.ANY), vmem),
         scratch_shapes=sems,
         compiler_params=pltpu.CompilerParams(collective_id=0, has_side_effects=True),
         cost_estimate=pl.CostEstimate(
             flops=30_000_000_000, bytes_accessed=10_000_000, transcendentals=0
         ),
         name="dispatch",
-    )(own)
+    )(own, tail)
 
 
 def combine(parts, mix_parts, n):
@@ -289,15 +311,6 @@
     tokens = c_gate.shape[0]
     reach = conv_taps.shape[0] - 1
     product = c_gate.astype(jnp.float32) * values.astype(jnp.float32)
-    previous = passed_along(product[tokens - reach :], "ep", 1)
-    extended = jnp.concatenate([previous, product], 0)
-    convolved = jnp.zeros_like(product)
-    for offset in range(reach + 1):
-        convolved = convolved + conv_taps[offset][None, :] * extended[offset : offset + tokens]
-    mixed = (b_gate.astype(jnp.float32) * convolved).astype(jnp.bfloat16)
-    mix_parts = jnp.dot(mixed, w_mix_out, preferred_element_type=jnp.float32).astype(jnp.bfloat16)
-    mix_parts = mix_parts.reshape(n_tp, tokens // n_tp, -1)
-
     rows_b = moe_in.shape[0]
     width = moe_in.shape[1]
     top = route_ids.shape[1]
@@ -325,7 +338,18 @@
     select = placed.astype(jnp.bfloat16).reshape(experts * capacity, rows_b)
     own = jnp.dot(select, normed, preferred_element_type=jnp.float32).astype(jnp.bfloat16)
 
-    piece = dispatch(own.reshape(experts, capacity, width), n_ep).reshape(-1, width)
+    arrived, previous = dispatch(
+        own.reshape(experts, capacity, width), product[tokens - reach :], n_ep
+    )
+    piece = arrived.reshape(-1, width)
+    previous = jnp.where(lax.axis_index("ep") == 0, 0.0, previous)
+    extended = jnp.concatenate([previous, product], 0)
+    convolved = jnp.zeros_like(product)
+    for offset in range(reach + 1):
+        convolved = convolved + conv_taps[offset][None, :] * extended[offset : offset + tokens]
+    mixed = (b_gate.astype(jnp.float32) * convolved).astype(jnp.bfloat16)
+    mix_parts = jnp.dot(mixed, w_mix_out, preferred_element_type=jnp.float32).astype(jnp.bfloat16)
+    mix_parts = mix_parts.reshape(n_tp, tokens // n_tp, -1)
     gate_val = jnp.dot(piece, w_gate[0], preferred_element_type=jnp.float32)
     up_val = jnp.dot(piece, w_up[0], preferred_element_type=jnp.float32)
     hidden = (jax.nn.silu(gate_val) * up_val).astype(jnp.bfloat16)

time: 143 us -> 141 us (0.986)
  starting transfers between devices: 4.9 us -> 0 us
  Pallas kernels: 95.9 us -> 98.6 us
    ppermute x1 -> x0, starting transfers between devices: 4.9 us -> none  [passed_along(): return lax.ppermute(block, axis, route)]
    pallas_call x1, Pallas kernels: 46.5 us -> 48.5 us  [dispatch(): pl.pallas_call(functools.partial(dispatch_kernel, n), out_shape=(jax.Shap...]
  transfers between devices with their start and end apart: 1 -> 0, of which waited for: 0 -> 0; matrix products, arithmetic and copies ran while one was open for 23% -> 0% of each run, Pallas kernels for 33% -> 0%
where the time goes in v2:
time: 141 us; the launch traced here: 140 us
  Pallas kernels  98.6 us (70%)
  matrix products  36.2 us (26%)
  other arithmetic  2.37 us (2%)
  local copies, waits for them, and re-layouts  2.19 us (2%)
    pallas_call x1, Pallas kernels, combine(): pl.pallas_call(functools.partial(combine_kernel, n), out_shape=(jax.Shape...  50.1 us
    pallas_call x1, Pallas kernels, dispatch(): pl.pallas_call(functools.partial(dispatch_kernel, n), out_shape=(jax.Shap...  48.5 us
    dot_general x1, matrix products, on_device(): jnp.dot(hidden, w_down[0], preferred_element_type=jnp.float32)  17.5 us
    dot_general x1, matrix products, on_device(): gate_val = jnp.dot(piece, w_gate[0], preferred_element_type=jnp.float32)  9.96 us

profile of v2, /device:TPU:0, one launch (start us, length us, event | category | flops | bytes accessed | tf_op | source)
XLA Modules:
  0.0 140.1 jit_solution(7613833092299984147)
XLA Ops:
  0.6 0.0 copy-start
  0.6 0.8 slice_bitcast_fusion.3
  1.4 0.1 convolution_convert_fusion.3
  1.6 0.1 eq.85
  1.7 0.1 fusion.21
  1.8 1.2 fusion.6
  3.0 2.7 %convolution_convert_fusion.1 = bf16[320,2048]{1,0:T(8,128)(2,1)} fusion(pred[320,128]{1,0:T(32,128)(4,1)S(1)} %fusion.21, bf16[128,2048]{1,0:T(8,128)(2,1)} %param.17, f32[2048]{0:T(1024)} %param.18, f32[128]{0:T(128)S(1)} %add_rsqrt_fusion), kind=kOutput, calls=%fused_computation.6 | convolution fusion | flops 169476096 | bytes 1884672 | tf_op jit(solution)/shard_map/dot_general | solution.py:339
  5.7 1.0 convert_multiply_fusion.2
  6.7 0.6 slice.40.tail
  7.3 48.5 %dispatch.1 = (bf16[4,8,40,2048]{3,2,1,0:T(8,128)(2,1)}, f32[2,256]{1,0:T(2,128)}) custom-call(bf16[8,40,2048]{2,1,0:T(8,128)(2,1)} %bitcast.55, f32[2,256]{1,0:T(2,128)} %slice.40.tail), custom_call_target="tpu_custom_call" | custom-call | flops 30000001024 | bytes 10000000 | tf_op jit(solution)/shard_map/dispatch/pallas_call | solution.py:249
  55.8 10.0 %fusion.2 = f32[1280,896]{1,0:T(8,128)} fusion(bf16[1280,2048]{1,0:T(8,128)(2,1)} %bitcast.59, bf16[1,2048,896]{2,1,0:T(8,128)(2,1)} %param.21), kind=kOutput, calls=%fused_computation.4 | convolution fusion | flops 4697620480 | bytes 13500416 | tf_op jit(solution)/shard_map/dot_general | solution.py:353
  65.8 0.0 copy-start.4
  65.8 0.0 copy-start.3
  65.8 0.0 copy-start.2
  65.8 17.5 %convolution_convert_fusion = bf16[1280,2048]{1,0:T(8,128)(2,1)} fusion(bf16[1,896,2048]{2,1,0:T(8,128)(2,1)} %param.23, f32[1280,896]{1,0:T(8,128)} %fusion.2, bf16[1280,2048]{1,0:T(8,128)(2,1)} %bitcast.60, bf16[1,2048,896]{2,1,0:T(8,128)(2,1)} %param.22), kind=kOutput, calls=%fused_computation | convolution fusion | flops 9404743680 | bytes 22413312 | tf_op jit(solution)/shard_map/dot_general | solution.py:356
  83.3 0.0 copy-done.4
  83.3 0.0 copy-done.3
  83.4 0.0 copy-done
  83.4 0.0 copy-done.2
  83.4 1.5 %convolution_convert_fusion.2 = bf16[256,2048]{1,0:T(8,128)(2,1)} fusion(bf16[256,2048]{1,0:T(8,128)(2,1)S(1)} %copy-done, f32[2,256]{1,0:T(2,128)S(1)} %broadcast_select_fusion, f32[256,256]{1,0:T(8,128)S(1)} %convert_multiply_fusion.2, bf16[256,256]{1,0:T(8,128)(2,1)S(1)} %copy-done.2, f32[256]{0:T(256)S(1)} %bitcast.57, f32[256]{0:T(256)S(1)} %bitcast.58, ...), kind=kOutput, calls=%fused_computation.7 | convolution fusion | flops 269615104 | bytes 2495488 | tf_op jit(solution)/shard_map/dot_general | solution.py:351
  84.8 0.0 copy-start.5
  84.8 50.1 %combine.1 = (bf16[8,40,2048]{2,1,0:T(8,128)(2,1)}, bf16[64,2048]{1,0:T(8,128)(2,1)}) custom-call(bf16[4,8,40,2048]{3,2,1,0:T(8,128)(2,1)} %bitcast.53, bf16[4,64,2048]{2,1,0:T(8,128)(2,1)} %bitcast.54), custom_call_target="tpu_custom_call" | custom-call | tf_op jit(solution)/shard_map/combine/pallas_call | solution.py:271
  134.9 0.0 copy-start.1
  134.9 0.0 copy-done.5
  135.0 1.8 %convolution_bitcast_fusion = f32[128,2048]{1,0:T(8,128)S(1)} fusion(bf16[8,40,2048]{2,1,0:T(8,128)(2,1)} %get-tuple-element.9, f32[8,128]{1,0:T(8,128)S(1)} %select_add_fusion, s32[8,128]{1,0:T(8,128)S(1)} %convolution_convert_fusion.3, pred[8,128]{1,0:T(8,128)(4,1)S(1)} %fusion.35), kind=kOutput, calls=%fused_computation.8 | convolution fusion | flops 168017920 | bytes 2368512 | tf_op jit(solution)/shard_map/dot_general | solution.py:368
  136.8 2.6 %fusion.5 = bf16[128,2048]{1,0:T(8,128)(2,1)} fusion(f32[128,2048]{1,0:T(8,128)S(1)} %convolution_bitcast_fusion, bf16[8,40,2048]{2,1,0:T(8,128)(2,1)} %get-tuple-element.9, f32[8,128]{1,0:T(8,128)S(1)} %select_add_fusion, s32[8,128]{1,0:T(8,128)S(1)} %convolution_convert_fusion.3, pred[8,128]{1,0:T(8,128)(4,1)S(1)} %fusion.35), kind=kOutput, calls=%fused_computation.11 | convolution fusion | flops 168501248 | bytes 2892800 | tf_op jit(solution)/shard_map/dot_general | solution.py:366
  139.4 0.0 copy-done.1
  139.4 0.7 copy.17
  (7 shorter events, 0.0 us)
Async XLA Ops:
  0.6 82.7 %copy-start = (bf16[256,2048]{1,0:T(8,128)(2,1)S(1)}, bf16[256,2048]{1,0:T(8,128)(2,1)}, u32[]{:S(2)}) copy-start(bf16[256,2048]{1,0:T(8,128)(2,1)} %param.16) | copy-start | bytes 3145732
  65.8 17.5 %copy-start.4 = (f32[2,256]{1,0:T(2,128)S(1)}, f32[2,256]{1,0:T(2,128)}, u32[]{:S(2)}) copy-start(f32[2,256]{1,0:T(2,128)} %get-tuple-element.7) | copy-start | bytes 6148
  65.8 17.6 %copy-start.3 = (f32[3,256]{1,0:T(4,128)S(1)}, f32[3,256]{1,0:T(4,128)}, u32[]{:S(2)}) copy-start(f32[3,256]{1,0:T(4,128)} %param.15) | copy-start | bytes 9220
  65.8 17.6 %copy-start.2 = (bf16[256,256]{1,0:T(8,128)(2,1)S(1)}, bf16[256,256]{1,0:T(8,128)(2,1)}, u32[]{:S(2)}) copy-start(bf16[256,256]{1,0:T(8,128)(2,1)} %param.13) | copy-start | bytes 393220
  84.8 50.1 %copy-start.5 = (f32[128,2]{0,1:T(2,128)S(1)}, f32[128,2]{0,1:T(2,128)}, u32[]{:S(2)}) copy-start(f32[128,2]{0,1:T(2,128)} %param.20) | copy-start | bytes 3076
  134.9 4.5 %copy-start.1 = (bf16[64,2048]{1,0:T(8,128)(2,1)S(1)}, bf16[64,2048]{1,0:T(8,128)(2,1)}, u32[]{:S(2)}) copy-start(bf16[64,2048]{1,0:T(8,128)(2,1)} %get-tuple-element.19) | copy-start | bytes 786436
